TPU v7x, 128 devices: a whole 4x4x4 slice. The times are simulated.
128 devices in a mesh: sp: 64 (over z, y, x), tp: 2 (over core).
Axes of the slice: x: 4, y: 4, z: 4, core: 2. Of those that a mesh axis runs over, the one named last changes fastest.
Arguments:
- queries: bfloat16 [8192, 1024], P('sp', 'tp'), may hold values from -6 to 6
- keys: bfloat16 [8192, 1024], P('sp', 'tp'), may hold values from -6 to 6
- values: bfloat16 [8192, 2048], P('sp', 'tp'), may hold values from -6 to 6
- out_gate: bfloat16 [8192, 2048], P('sp', 'tp'), may hold values from -6 to 6
- decay_rate: float32 [8], P('tp'), may hold values from 0 to 1
- residual: bfloat16 [8192, 2048], P(('sp', 'tp')), may hold values from -6 to 6
- out_weight: bfloat16 [2048, 2048], P('tp'), may hold values from -0.125 to 0.125
- ffn_gain: float32 [2048], replicated, may hold values from 0.1 to 1.9
- route_ids: int32 [8192, 4], P(('sp', 'tp')), may hold values from 0 to 63, all different within a row; in each aligned block of 64 rows (0 to 63, 64 to 127, ...) at most 8 rows name the same one
- route_weights: float32 [8192, 4], P(('sp', 'tp')), may hold values from 0.1 to 1
- gate_up: bfloat16 [64, 2048, 2048], P('sp', None, 'tp'), may hold values from -0.375 to 0.375
- lin_up: bfloat16 [64, 2048, 2048], P('sp', None, 'tp'), may hold values from -0.375 to 0.375
- down_weight: bfloat16 [64, 2048, 2048], P('sp', 'tp'), may hold values from -0.03125 to 0.03125
Outputs:
- layer_out: bfloat16 [8192, 2048], P(('sp', 'tp'))
Inputs may be any that keep to these rules, and one draw needn't show every extreme that they name: `route_ids`: within the rows of one device (aligned blocks of 64 rows), no expert is named by more than 8 entries, a bound that some block reaches; the 4 experts of a row differ.
All inputs are finite; a program needn't handle non-finite values.
Results may differ from a plain program's by a relative error of at most 0.03.
Values may be sent and summed in bfloat16 or wider, within the bound.
A program may use at most 128 MiB of HBM per device.

v0:
```python
import jax
import jax.numpy as jnp
from jax import lax
from jax.sharding import Mesh
from jax.sharding import PartitionSpec as P

D = 2048
DK = 128
DV = 256
SP = ("sp_0", "sp_1", "sp_2")
SP_TP = ("sp_0", "sp_1", "sp_2", "tp")
EPS = 1e-05
CLAMP_LIMIT = 7.0
SIGMOID_SLOPE = 1.702
TOP_PRECISION = lax.Precision.HIGHEST


def carried_state(state_delta, log_gamma, block_len):
    peers, mine = (lax.axis_size(SP), lax.axis_index(SP))
    heads = state_delta.shape[0]
    pieces = state_delta.astype(jnp.bfloat16).reshape(peers, -1)
    arrived = lax.all_to_all(pieces, SP, split_axis=0, concat_axis=0, tiled=True)
    own_log = lax.dynamic_index_in_dim(log_gamma, mine * heads // peers, keepdims=False)
    order = jnp.arange(peers, dtype=jnp.float32)
    gap = order[:, None] - 1.0 - order[None, :]
    weight = jnp.where(gap >= 0, jnp.exp(jnp.maximum(gap, 0.0) * block_len * own_log), 0.0)
    before = jnp.dot(weight, arrived.astype(jnp.float32), precision=TOP_PRECISION)
    returned = lax.all_to_all(
        before.astype(jnp.bfloat16), SP, split_axis=0, concat_axis=0, tiled=True
    )
    return returned.reshape(state_delta.shape).astype(jnp.float32)


def in_blocks(array, dim, peers):
    before, after = (array.shape[:dim], array.shape[dim + 1 :])
    return jnp.moveaxis(array.reshape(*before, peers, -1, *after), dim, 0)


def summed_on_arrival(array, axis, dim):
    tiles = in_blocks(array, dim, lax.axis_size(axis))
    arrived = lax.all_to_all(tiles, axis, split_axis=0, concat_axis=0, tiled=True)
    return arrived.astype(jnp.float32).sum(axis=0)


def expert_act(row_block, gate_part, lin_part):
    gate_pre = jnp.dot(row_block, gate_part, preferred_element_type=jnp.float32)
    lin_pre = jnp.dot(row_block, lin_part, preferred_element_type=jnp.float32)
    gate_clip = jnp.minimum(gate_pre, CLAMP_LIMIT)
    lin_clip = jnp.clip(lin_pre, -CLAMP_LIMIT, CLAMP_LIMIT)
    return (gate_clip * jax.nn.sigmoid(SIGMOID_SLOPE * gate_clip) * (lin_clip + 1.0)).astype(
        jnp.bfloat16
    )


def local(
    queries,
    keys,
    values,
    out_gate,
    decay_rate,
    residual,
    out_weight,
    ffn_gain,
    route_ids,
    route_weights,
    gate_up,
    lin_up,
    down_weight,
):
    block_len = queries.shape[0]
    local_heads = decay_rate.shape[0]
    log_gamma = -decay_rate
    query_heads = queries.astype(jnp.float32).reshape(block_len, local_heads, DK).transpose(1, 0, 2)
    per_head_keys = keys.astype(jnp.float32).reshape(block_len, local_heads, DK).transpose(
        1, 0, 2
    ) * DK ** (-0.5)
    per_head_values = (
        values.astype(jnp.float32).reshape(block_len, local_heads, DV).transpose(1, 0, 2)
    )
    positions = jnp.arange(block_len, dtype=jnp.float32)
    offsets = positions[:, None] - positions[None, :]
    causal = offsets >= 0
    decay_mask = jnp.where(
        causal[None], jnp.exp(jnp.where(causal, offsets, 0.0)[None] * log_gamma[:, None, None]), 0.0
    )
    trailing_decay = jnp.exp((block_len - 1.0 - positions)[None, :] * log_gamma[:, None])
    lead_decay = jnp.exp((positions + 1.0)[None, :] * log_gamma[:, None])
    attention_scores = (
        jnp.einsum("hqd,hkd->hqk", query_heads, per_head_keys, precision=TOP_PRECISION) * decay_mask
    )
    intra_block_term = jnp.einsum(
        "zfp,zpn->zfn", attention_scores, per_head_values, precision=TOP_PRECISION
    )
    state_delta = jnp.einsum(
        "mxs,mxq->msq",
        per_head_keys * trailing_decay[:, :, None],
        per_head_values,
        precision=TOP_PRECISION,
    )
    carried = carried_state(state_delta, log_gamma, block_len)
    cross_term = (
        jnp.einsum("hqd,hdv->hqv", query_heads, carried, precision=TOP_PRECISION)
        * lead_decay[:, :, None]
    )
    retained = intra_block_term + cross_term
    normed = retained * lax.rsqrt(jnp.mean(retained * retained, axis=-1, keepdims=True) + EPS)
    gated = (
        normed.transpose(1, 0, 2).reshape(block_len, local_heads * DV)
        * jax.nn.silu(out_gate.astype(jnp.float32))
    ).astype(jnp.bfloat16)
    mix_rows = summed_on_arrival(
        jnp.dot(gated, out_weight, preferred_element_type=jnp.float32).astype(jnp.bfloat16), "tp", 0
    )
    mixed = (residual.astype(jnp.float32) + mix_rows).astype(jnp.bfloat16)
    mixed_wide = mixed.astype(jnp.float32)
    normed_rows = (
        mixed_wide
        * lax.rsqrt(jnp.mean(mixed_wide * mixed_wide, axis=-1, keepdims=True) + EPS)
        * ffn_gain
    ).astype(jnp.bfloat16)
    experts = lax.axis_size(SP)
    own_rows = route_ids.shape[0]
    top_count = route_ids.shape[1]
    capacity = own_rows * top_count * lax.axis_size("tp") // experts
    flat_ids = route_ids.reshape(-1)
    one_hot = (flat_ids[:, None] == jnp.arange(experts, dtype=jnp.int32)[None, :]).astype(jnp.int32)
    slot_rank = jnp.sum(one_hot * (jnp.cumsum(one_hot, axis=0) - 1), axis=1)
    slot_index = flat_ids * capacity + slot_rank
    source_row = jnp.arange(own_rows * top_count, dtype=jnp.int32) // top_count
    slot_source = (
        jnp.full((experts * capacity,), own_rows, jnp.int32).at[slot_index].set(source_row)
    )
    padded = jnp.concatenate([normed_rows, jnp.zeros((1, D), jnp.bfloat16)], axis=0)
    outgoing = padded[slot_source].reshape(experts, capacity, D)
    gate_half = gate_up[0]
    lin_half = lin_up[0]
    down_half = down_weight[0]
    pair_rows = lax.all_gather(
        lax.all_to_all(outgoing, SP, split_axis=0, concat_axis=0, tiled=True),
        "tp",
        axis=0,
        tiled=True,
    )
    activation = expert_act(pair_rows.reshape(-1, D), gate_half, lin_half)
    partial_value = jnp.dot(activation, down_half, preferred_element_type=jnp.float32).reshape(
        pair_rows.shape
    )
    summed = summed_on_arrival(partial_value.astype(jnp.bfloat16), "tp", 0)
    returned = lax.all_to_all(
        summed.astype(jnp.bfloat16), SP, split_axis=0, concat_axis=0, tiled=True
    )
    picked = (
        returned.reshape(experts * capacity, D)[slot_index]
        .reshape(own_rows, top_count, D)
        .astype(jnp.float32)
    )
    expert_sum = jnp.sum(picked * route_weights[:, :, None], axis=1)
    return (mixed_wide + expert_sum).astype(jnp.bfloat16)


def solution(mesh):
    torus = Mesh(mesh.devices.reshape(4, 4, 4, mesh.shape["tp"]), ("sp_0", "sp_1", "sp_2", "tp"))
    in_specs = (
        P(SP, "tp"),
        P(SP, "tp"),
        P(SP, "tp"),
        P(SP, "tp"),
        P("tp"),
        P(SP_TP, None),
        P("tp", None),
        P(),
        P(SP_TP, None),
        P(SP_TP, None),
        P(SP, None, "tp"),
        P(SP, None, "tp"),
        P(SP, "tp", None),
    )
    out_specs = P(SP_TP, None)
    return jax.shard_map(local, mesh=torus, in_specs=in_specs, out_specs=out_specs, check_vma=False)
```

profile of v0, /device:TPU:0, one launch (start us, length us, event | category | flops | bytes accessed | tf_op | source)
XLA Modules:
  0.0 202.1 jit_solution(13798051839371577354)
XLA Ops:
  6.5 0.7 neg.10
  7.3 1.0 copy.102
  8.3 1.3 convolution_convert_fusion.2
  10.4 2.2 %reduce.4 = bf16[64,2048]{1,0:T(8,128)(2,1)S(1)} reduce(bf16[64,1,2048]{2,1,0:T(2,128)(2,1)S(1)} %all_to_all.35, bf16[]{:T(256)} %broadcast.223), dimensions={1}, to_apply=%all_to_all.35.reduce_sub_computation | reduce | bytes 524290 | tf_op jit(solution)/shard_map/all_to_all | solution.py:22
  12.6 0.9 reshape.247
  13.5 11.7 %all-to-all-start = ((bf16[64,2,1024]{2,1,0:T(2,128)(2,1)}), bf16[64,2,1024]{2,1,0:T(2,128)(2,1)S(1)}, u32[]{:S(2)}, u32[]{:S(2)}) async-start(bf16[64,2,1024]{2,1,0:T(2,128)(2,1)} %reshape.247), calls=%async_computation | async-start | bytes 524288 | tf_op jit(solution)/shard_map/all_to_all | solution.py:22
  25.3 0.8 copy.90
  29.3 1.4 scatter_custom_fusion
  30.8 5.0 %all-to-all-done = bf16[64,2,1024]{2,1,0:T(2,128)(2,1)S(1)} async-done(((bf16[64,2,1024]{2,1,0:T(2,128)(2,1)}), bf16[64,2,1024]{2,1,0:T(2,128)(2,1)S(1)}, u32[]{:S(2)}, u32[]{:S(2)}) %all-to-all-start) | async-done | bytes 262176 | tf_op jit(solution)/shard_map/all_to_all | solution.py:22
  36.5 0.8 reduce.5
  37.3 0.9 reshape.249
  38.2 5.4 %all-to-all-start.1 = ((bf16[64,2,1024]{2,1,0:T(2,128)(2,1)}), bf16[64,2,1024]{2,1,0:T(2,128)(2,1)S(1)}, u32[]{:S(2)}, u32[]{:S(2)}) async-start(bf16[64,2,1024]{2,1,0:T(2,128)(2,1)} %reshape.249), calls=%async_computation.1 | async-start | bytes 524288 | tf_op jit(solution)/shard_map/all_to_all | solution.py:28
  44.2 10.0 %all-to-all-done.1 = bf16[64,2,1024]{2,1,0:T(2,128)(2,1)S(1)} async-done(((bf16[64,2,1024]{2,1,0:T(2,128)(2,1)}), bf16[64,2,1024]{2,1,0:T(2,128)(2,1)S(1)}, u32[]{:S(2)}, u32[]{:S(2)}) %all-to-all-start.1) | async-done | bytes 262176 | tf_op jit(solution)/shard_map/all_to_all | solution.py:28
  54.4 1.5 reduce.1
  57.4 2.9 %convolution_convert_fusion = bf16[128,2048]{1,0:T(8,128)(2,1)S(1)} fusion(bf16[128,1024]{0,1:T(8,128)(2,1)S(1)} %fusion.35, bf16[1024,2048]{1,0:T(8,128)(2,1)} %param.19), kind=kOutput, calls=%fused_computation.13 | convolution fusion | flops 537133056 | bytes 4980736 | tf_op jit(solution)/shard_map/dot_general | solution.py:112
  60.3 4.2 %all_to_all.42 = bf16[2,64,2048]{2,1,0:T(8,128)(2,1)S(1)} all-to-all(bf16[2,64,2048]{2,1,0:T(8,128)(2,1)S(1)} %bitcast.118), channel_id=1, replica_groups=mesh['sp_0'=4,'sp_1'=4,'sp_2'=4,'tp'=2] {'tp'}, dimensions={0} | all-to-all | bytes 1048576 | tf_op jit(solution)/shard_map/all_to_all | solution.py:41
  65.0 2.5 %gather_fusion = bf16[512,2048]{1,0:T(8,128)(2,1)S(1)} fusion(bf16[65,2048]{1,0:T(8,128)(2,1)S(1)} %concatenate.3, s32[1024]{0:T(1024)S(1)} %pad_clamp_fusion.1), kind=kCustom, calls=%fused_computation | custom fusion | bytes 4196352 | tf_op jit(solution)/shard_map/gather | solution.py:134
  67.4 35.2 %all_to_all.43 = bf16[64,8,2048]{2,1,0:T(8,128)(2,1)} all-to-all(bf16[64,8,2048]{2,1,0:T(8,128)(2,1)S(1)} %bitcast.114), channel_id=1, replica_groups=mesh['sp_0'=4,'sp_1'=4,'sp_2'=4,'tp'=2] {'sp_0','sp_1','sp_2'}, dimensions={0} | all-to-all | bytes 4194304 | tf_op jit(solution)/shard_map/all_to_all | solution.py:139
  102.7 13.1 %all-gather.2.cloned.1.call-done = bf16[128,8,2048]{2,1,0:T(8,128)(2,1)} async-done(((bf16[64,8,2048]{2,1,0:T(8,128)(2,1)}), bf16[128,8,2048]{2,1,0:T(8,128)(2,1)}) %all-gather.2.cloned.1.call-update) | async-done | bytes 4194320 | tf_op jit(solution)/shard_map/all_gather | solution.py:138
  115.8 7.6 %fusion.2 = f32[1024,1024]{1,0:T(8,128)S(1)} fusion(bf16[1,2048,1024]{2,1,0:T(8,128)(2,1)} %param.24, bf16[128,8,2048]{2,1,0:T(8,128)(2,1)} %all-gather.2.cloned.1.call-done), kind=kOutput, calls=%fused_computation.5 | convolution fusion | flops 4294967296 | bytes 12582912 | tf_op jit(solution)/shard_map/dot_general | solution.py:47
  123.5 5.8 %fusion.17 = bf16[128,8,1024]{2,1,0:T(8,128)(2,1)S(1)} fusion(f32[1024,1024]{1,0:T(8,128)S(1)} %fusion.2, bf16[1,2048,1024]{2,1,0:T(8,128)(2,1)S(1)} %copy-done.6, bf16[128,8,2048]{2,1,0:T(8,128)(2,1)S(1)} %copy-done.8), kind=kOutput, calls=%fused_computation.18 | convolution fusion | flops 4305453056 | bytes 14680064 | tf_op jit(solution)/shard_map/dot_general | solution.py:46
  129.3 5.2 %fusion.8 = bf16[128,8,2048]{2,0,1:T(8,128)(2,1)S(1)} fusion(bf16[1,1024,2048]{2,1,0:T(8,128)(2,1)S(1)} %copy-done.7, bf16[128,8,1024]{2,1,0:T(8,128)(2,1)S(1)} %fusion.17), kind=kOutput, calls=%fused_computation.12 | convolution fusion | flops 4297064448 | bytes 10485760 | tf_op jit(solution)/shard_map/dot_general | solution.py:145
  135.1 8.2 %all_to_all.44 = bf16[2,64,8,2048]{3,1,2,0:T(8,128)(2,1)} all-to-all(bf16[2,64,8,2048]{3,1,2,0:T(8,128)(2,1)S(1)} %copy.94), channel_id=1, replica_groups=mesh['sp_0'=4,'sp_1'=4,'sp_2'=4,'tp'=2] {'tp'}, dimensions={0} | all-to-all | bytes 8388608 | tf_op jit(solution)/shard_map/all_to_all | solution.py:41
  143.2 3.5 %reduce_sum.64 = bf16[64,8,2048]{2,0,1:T(8,128)(2,1)S(1)} reduce(bf16[2,64,8,2048]{3,1,2,0:T(8,128)(2,1)} %all_to_all.44, bf16[]{:T(256)} %constant.96.clone.1), dimensions={0}, to_apply=%region_7.8 | reduce | flops 1048576 | bytes 6291458 | tf_op jit(solution)/shard_map/reduce_sum | solution.py:42
  146.7 2.5 %copy.96 = bf16[64,8,2048]{2,1,0:T(8,128)(2,1)} copy(bf16[64,8,2048]{2,0,1:T(8,128)(2,1)S(1)} %reduce_sum.64) | data formatting | bytes 4194304 | tf_op jit(solution)/shard_map/reduce_sum | solution.py:42
  149.2 10.6 %all-to-all-start.5 = ((bf16[64,8,2048]{2,1,0:T(8,128)(2,1)}), bf16[64,8,2048]{2,1,0:T(8,128)(2,1)S(1)}, u32[]{:S(2)}, u32[]{:S(2)}) async-start(bf16[64,8,2048]{2,1,0:T(8,128)(2,1)} %copy.96), calls=%async_computation.5 | async-start | bytes 4194304 | tf_op jit(solution)/shard_map/all_to_all | solution.py:149
  159.9 0.7 copy.97
  160.6 29.4 %all-to-all-done.5 = bf16[64,8,2048]{2,1,0:T(8,128)(2,1)S(1)} async-done(((bf16[64,8,2048]{2,1,0:T(8,128)(2,1)}), bf16[64,8,2048]{2,1,0:T(8,128)(2,1)S(1)}, u32[]{:S(2)}, u32[]{:S(2)}) %all-to-all-start.5) | async-done | bytes 2097184 | tf_op jit(solution)/shard_map/all_to_all | solution.py:149
  190.0 1.4 gather_fusion.1
  191.4 0.7 reshape.215
  192.1 2.4 %multiply_reduce_fusion = f32[64,2048]{1,0:T(8,128)S(1)} fusion(f32[64,4,2048]{2,1,0:T(4,128)S(1)} %reshape.215, f32[64,4]{1,0:T(8,128)} %copy.97), kind=kLoop, calls=%fused_computation.17 | loop fusion | flops 917504 | bytes 2622464 | tf_op jit(solution)/shard_map/reduce_sum | solution.py:157
  194.5 0.8 fusion.30
  (63 shorter events, 7.6 us)
Async XLA Ops:
  6.5 37.3 %copy-start = (bf16[128,512]{1,0:T(8,128)(2,1)S(1)}, bf16[128,512]{1,0:T(8,128)(2,1)}, u32[]{:S(2)}) copy-start(bf16[128,512]{1,0:T(8,128)(2,1)} %param.13) | copy-start | bytes 393220
  6.5 37.1 %copy-start.2 = (bf16[128,1024]{1,0:T(8,128)(2,1)S(1)}, bf16[128,1024]{1,0:T(8,128)(2,1)}, u32[]{:S(2)}) copy-start(bf16[128,1024]{1,0:T(8,128)(2,1)} %param.16) | copy-start | bytes 786436
  13.5 42.8 %copy-start.1 = (bf16[128,1024]{1,0:T(8,128)(2,1)S(1)}, bf16[128,1024]{1,0:T(8,128)(2,1)}, u32[]{:S(2)}) copy-start(bf16[128,1024]{1,0:T(8,128)(2,1)} %param.15) | copy-start | bytes 786436
  13.5 22.3 %all-to-all-start = ((bf16[64,2,1024]{2,1,0:T(2,128)(2,1)}), bf16[64,2,1024]{2,1,0:T(2,128)(2,1)S(1)}, u32[]{:S(2)}, u32[]{:S(2)}) async-start(bf16[64,2,1024]{2,1,0:T(2,128)(2,1)} %reshape.247), calls=%async_computation | async-start | bytes 524288 | tf_op jit(solution)/shard_map/all_to_all | solution.py:22
  38.2 16.0 %all-to-all-start.1 = ((bf16[64,2,1024]{2,1,0:T(2,128)(2,1)}), bf16[64,2,1024]{2,1,0:T(2,128)(2,1)S(1)}, u32[]{:S(2)}, u32[]{:S(2)}) async-start(bf16[64,2,1024]{2,1,0:T(2,128)(2,1)} %reshape.249), calls=%async_computation.1 | async-start | bytes 524288 | tf_op jit(solution)/shard_map/all_to_all | solution.py:28
  43.5 72.3 %all-gather.2.cloned.1.call-start = ((), (), s32[]{:S(2)}) async-start(), calls=%async_computation.6 | async-start | bytes 6291456 | tf_op jit(solution)/shard_map/all_gather | solution.py:138
  57.2 7.4 %copy-start.3 = (bf16[64,2048]{1,0:T(8,128)(2,1)S(1)}, bf16[64,2048]{1,0:T(8,128)(2,1)}, u32[]{:S(2)}) copy-start(bf16[64,2048]{1,0:T(8,128)(2,1)} %param.18) | copy-start | bytes 786436
  57.4 7.4 %copy-start.4 = (f32[2048]{0:T(1024)S(1)}, f32[2048]{0:T(1024)}, u32[]{:S(2)}) copy-start(f32[2048]{0:T(1024)} %param.20) | copy-start | bytes 24580
  115.8 7.7 %copy-start.6 = (bf16[1,2048,1024]{2,1,0:T(8,128)(2,1)S(1)}, bf16[1,2048,1024]{2,1,0:T(8,128)(2,1)}, u32[]{:S(2)}) copy-start(bf16[1,2048,1024]{2,1,0:T(8,128)(2,1)} %param.23) | copy-start | bytes 12582916
  115.8 7.7 %copy-start.8 = (bf16[128,8,2048]{2,1,0:T(8,128)(2,1)S(1)}, bf16[128,8,2048]{2,1,0:T(8,128)(2,1)}, u32[]{:S(2)}) copy-start(bf16[128,8,2048]{2,1,0:T(8,128)(2,1)} %all-gather.2.cloned.1.call-done) | copy-start | bytes 12582916
  123.5 5.8 %copy-start.7 = (bf16[1,1024,2048]{2,1,0:T(8,128)(2,1)S(1)}, bf16[1,1024,2048]{2,1,0:T(8,128)(2,1)}, u32[]{:S(2)}) copy-start(bf16[1,1024,2048]{2,1,0:T(8,128)(2,1)} %param.25) | copy-start | bytes 12582916
  146.7 13.1 %copy-start.5 = (f32[64,4]{0,1:T(4,128)S(1)}, f32[64,4]{0,1:T(4,128)}, u32[]{:S(2)}) copy-start(f32[64,4]{0,1:T(4,128)} %param.22) | copy-start | bytes 3076
  149.2 40.8 %all-to-all-start.5 = ((bf16[64,8,2048]{2,1,0:T(8,128)(2,1)}), bf16[64,8,2048]{2,1,0:T(8,128)(2,1)S(1)}, u32[]{:S(2)}, u32[]{:S(2)}) async-start(bf16[64,8,2048]{2,1,0:T(8,128)(2,1)} %copy.96), calls=%async_computation.5 | async-start | bytes 4194304 | tf_op jit(solution)/shard_map/all_to_all | solution.py:149
Sparse Core Ops, SparseCore 0:
  102.8 12.9 all-gather.1
where the time goes:
time: 203 us; the launch traced here: 202 us
  waiting for transfers between devices  57.5 us (28%)
  blocking collectives  47.6 us (23%)
  starting transfers between devices  27.7 us (14%)
  matrix products  24.4 us (12%)
  local copies, waits for them, and re-layouts  16.2 us (8%)
  between operations  14.4 us (7%)
  other arithmetic  14.3 us (7%)
    all_to_all x1, blocking collectives, local(): lax.all_to_all(outgoing, SP, split_axis=0, concat_axis=0, tiled=True)  35.2 us
    all_to_all x1, waiting for transfers between devices, local(): lax.all_to_all(summed.astype(jnp.bfloat16), SP, split_axis=0, concat_axis...  29.4 us
    all_gather x1, waiting for transfers between devices, local(): lax.all_gather(lax.all_to_all(outgoing, SP, split_axis=0, concat_axis=0,...  13.1 us
    all_to_all x2, blocking collectives, summed_on_arrival(): lax.all_to_all(tiles, axis, split_axis=0, concat_axis=0, tiled=True)  12.3 us
    all_to_all x1, starting transfers between devices, carried_state(): lax.all_to_all(pieces, SP, split_axis=0, concat_axis=0, tiled=True)  11.7 us
    all_to_all x1, starting transfers between devices, local(): lax.all_to_all(summed.astype(jnp.bfloat16), SP, split_axis=0, concat_axis...  10.6 us
    all_to_all x1, waiting for transfers between devices, carried_state(): lax.all_to_all(before.astype(jnp.bfloat16), SP, split_axis=0, concat_axis...  9.95 us
    dot_general x1, matrix products, expert_act(): lin_pre = jnp.dot(row_block, lin_part, preferred_element_type=jnp.float32)  7.65 us
  transfers between devices with their start and end apart: 4, of which 4 were waited for; matrix products, arithmetic and copies ran while one was open for 3% of the time, Pallas kernels for 0%

commit v1 on v0

--- a/solution.py
+++ b/solution.py
@@ -135,11 +135,17 @@
     gate_half = gate_up[0]
     lin_half = lin_up[0]
     down_half = down_weight[0]
-    pair_rows = lax.all_gather(
-        lax.all_to_all(outgoing, SP, split_axis=0, concat_axis=0, tiled=True),
-        "tp",
+    pair_rows = jnp.concatenate(
+        lax.all_to_all(
+            jnp.stack(
+                [lax.all_to_all(outgoing, SP, split_axis=0, concat_axis=0, tiled=True)]
+                * lax.axis_size("tp")
+            ),
+            "tp",
+            0,
+            0,
+        ),
         axis=0,
-        tiled=True,
     )
     activation = expert_act(pair_rows.reshape(-1, D), gate_half, lin_half)
     partial_value = jnp.dot(activation, down_half, preferred_element_type=jnp.float32).reshape(

time: 203 us -> 176 us (0.87)
  between operations: 14.4 us -> 1.02 us
  waiting for transfers between devices: 57.5 us -> 44.8 us
  blocking collectives: 47.6 us -> 54.8 us
  starting transfers between devices: 27.7 us -> 22.7 us
  matrix products: 24.4 us -> 21.3 us
    all_gather x1 -> x0, waiting for transfers between devices: 13.1 us -> none  [local(): lax.all_gather(lax.all_to_all(outgoing, SP, split_axis=0, concat_axis=0,...]
    all_to_all x0 -> x1, blocking collectives: none -> 7.37 us  [local(): lax.all_to_all(jnp.stack([lax.all_to_all(outgoing, SP, split_axis=0, conc...]
    all_to_all x1, starting transfers between devices: 10.6 us -> 5.67 us  [local(): lax.all_to_all(summed.astype(jnp.bfloat16), SP, split_axis=0, concat_axis...]
    dot_general x1, matrix products: 7.65 us -> 4.53 us  [expert_act(): lin_pre = jnp.dot(row_block, lin_part, preferred_element_type=jnp.float32)]
  transfers between devices with their start and end apart: 4 -> 3, of which waited for: 4 -> 3; matrix products, arithmetic and copies ran while one was open for 3% -> 4% of each run, Pallas kernels for 0% -> 0%
where the time goes in v1:
time: 176 us; the launch traced here: 175 us
  blocking collectives  54.8 us (31%)
  waiting for transfers between devices  44.8 us (25%)
  starting transfers between devices  22.7 us (13%)
  matrix products  21.3 us (12%)
  local copies, waits for them, and re-layouts  16.2 us (9%)
  other arithmetic  14.6 us (8%)
    all_to_all x1, blocking collectives, local(): lax.all_to_all(outgoing, SP, split_axis=0, concat_axis=0, tiled=True)  35.1 us
    all_to_all x1, waiting for transfers between devices, local(): lax.all_to_all(summed.astype(jnp.bfloat16), SP, split_axis=0, concat_axis...  29.8 us
    all_to_all x2, blocking collectives, summed_on_arrival(): lax.all_to_all(tiles, axis, split_axis=0, concat_axis=0, tiled=True)  12.3 us
    all_to_all x1, starting transfers between devices, carried_state(): lax.all_to_all(pieces, SP, split_axis=0, concat_axis=0, tiled=True)  11.7 us
    all_to_all x1, waiting for transfers between devices, carried_state(): lax.all_to_all(before.astype(jnp.bfloat16), SP, split_axis=0, concat_axis...  10 us
    all_to_all x1, blocking collectives, local(): lax.all_to_all(jnp.stack([lax.all_to_all(outgoing, SP, split_axis=0, conc...  7.37 us
    dot_general x1, matrix products, expert_act(): gate_pre = jnp.dot(row_block, gate_part, preferred_element_type=jnp.float32)  5.76 us
    all_to_all x1, starting transfers between devices, local(): lax.all_to_all(summed.astype(jnp.bfloat16), SP, split_axis=0, concat_axis...  5.67 us
  transfers between devices with their start and end apart: 3, of which 3 were waited for; matrix products, arithmetic and copies ran while one was open for 4% of the time, Pallas kernels for 0%

profile of v1, /device:TPU:0, one launch (start us, length us, event | category | flops | bytes accessed | tf_op | source)
XLA Modules:
  0.0 175.4 jit_solution(14057252559338758177)
XLA Ops:
  0.0 0.7 neg.10
  0.7 1.0 copy.102
  1.8 1.3 convolution_convert_fusion.2
  3.9 2.2 %reduce.4 = bf16[64,2048]{1,0:T(8,128)(2,1)S(1)} reduce(bf16[64,1,2048]{2,1,0:T(2,128)(2,1)S(1)} %all_to_all.39, bf16[]{:T(256)} %broadcast.223), dimensions={1}, to_apply=%all_to_all.39.reduce_sub_computation | reduce | bytes 524290 | tf_op jit(solution)/shard_map/all_to_all | solution.py:22
  6.1 0.9 reshape.243
  7.0 11.7 %all-to-all-start = ((bf16[64,2,1024]{2,1,0:T(2,128)(2,1)}), bf16[64,2,1024]{2,1,0:T(2,128)(2,1)S(1)}, u32[]{:S(2)}, u32[]{:S(2)}) async-start(bf16[64,2,1024]{2,1,0:T(2,128)(2,1)} %reshape.243), calls=%async_computation | async-start | bytes 524288 | tf_op jit(solution)/shard_map/all_to_all | solution.py:22
  18.8 0.8 copy.90
  22.8 1.4 scatter_custom_fusion
  24.2 5.0 %all-to-all-done = bf16[64,2,1024]{2,1,0:T(2,128)(2,1)S(1)} async-done(((bf16[64,2,1024]{2,1,0:T(2,128)(2,1)}), bf16[64,2,1024]{2,1,0:T(2,128)(2,1)S(1)}, u32[]{:S(2)}, u32[]{:S(2)}) %all-to-all-start) | async-done | bytes 262176 | tf_op jit(solution)/shard_map/all_to_all | solution.py:22
  29.9 0.8 reduce.5
  30.8 0.9 reshape.245
  31.6 5.4 %all-to-all-start.1 = ((bf16[64,2,1024]{2,1,0:T(2,128)(2,1)}), bf16[64,2,1024]{2,1,0:T(2,128)(2,1)S(1)}, u32[]{:S(2)}, u32[]{:S(2)}) async-start(bf16[64,2,1024]{2,1,0:T(2,128)(2,1)} %reshape.245), calls=%async_computation.1 | async-start | bytes 524288 | tf_op jit(solution)/shard_map/all_to_all | solution.py:28
  37.6 10.0 %all-to-all-done.1 = bf16[64,2,1024]{2,1,0:T(2,128)(2,1)S(1)} async-done(((bf16[64,2,1024]{2,1,0:T(2,128)(2,1)}), bf16[64,2,1024]{2,1,0:T(2,128)(2,1)S(1)}, u32[]{:S(2)}, u32[]{:S(2)}) %all-to-all-start.1) | async-done | bytes 262176 | tf_op jit(solution)/shard_map/all_to_all | solution.py:28
  47.8 1.5 reduce.1
  50.9 2.9 %convolution_convert_fusion = bf16[128,2048]{1,0:T(8,128)(2,1)S(1)} fusion(bf16[128,1024]{0,1:T(8,128)(2,1)S(1)} %fusion.29, bf16[1024,2048]{1,0:T(8,128)(2,1)} %param.19), kind=kOutput, calls=%fused_computation.12 | convolution fusion | flops 537133056 | bytes 4980736 | tf_op jit(solution)/shard_map/dot_general | solution.py:112
  53.8 4.2 %all_to_all.47 = bf16[2,64,2048]{2,1,0:T(8,128)(2,1)S(1)} all-to-all(bf16[2,64,2048]{2,1,0:T(8,128)(2,1)S(1)} %bitcast.116), channel_id=1, replica_groups=mesh['sp_0'=4,'sp_1'=4,'sp_2'=4,'tp'=2] {'tp'}, dimensions={0} | all-to-all | bytes 1048576 | tf_op jit(solution)/shard_map/all_to_all | solution.py:41
  58.4 2.5 %gather_fusion = bf16[512,2048]{1,0:T(8,128)(2,1)S(1)} fusion(bf16[65,2048]{1,0:T(8,128)(2,1)S(1)} %concatenate.3, s32[1024]{0:T(1024)S(1)} %pad_clamp_fusion.1), kind=kCustom, calls=%fused_computation | custom fusion | bytes 4196352 | tf_op jit(solution)/shard_map/gather | solution.py:134
  60.9 35.1 %all_to_all.48 = bf16[64,8,2048]{2,1,0:T(8,128)(2,1)S(1)} all-to-all(bf16[64,8,2048]{2,1,0:T(8,128)(2,1)S(1)} %bitcast.109), channel_id=1, replica_groups=mesh['sp_0'=4,'sp_1'=4,'sp_2'=4,'tp'=2] {'sp_0','sp_1','sp_2'}, dimensions={0} | all-to-all | bytes 4194304 | tf_op jit(solution)/shard_map/all_to_all | solution.py:141
  96.4 7.4 %all_to_all.49 = bf16[2,64,8,2048]{3,2,1,0:T(8,128)(2,1)S(1)} all-to-all(bf16[2,64,8,2048]{3,2,1,0:T(8,128)(2,1)S(1)} %pad_maximum_fusion), channel_id=1, replica_groups=mesh['sp_0'=4,'sp_1'=4,'sp_2'=4,'tp'=2] {'tp'}, dimensions={0} | all-to-all | bytes 8388608 | tf_op jit(solution)/shard_map/all_to_all | solution.py:139
  103.8 4.5 %fusion.2 = f32[1024,1024]{1,0:T(8,128)S(1)} fusion(bf16[1024,2048]{1,0:T(8,128)(2,1)S(1)} %bitcast.111, bf16[1,2048,1024]{2,1,0:T(8,128)(2,1)S(1)} %copy-done.7), kind=kOutput, calls=%fused_computation.6 | convolution fusion | flops 4294967296 | bytes 12582912 | tf_op jit(solution)/shard_map/dot_general | solution.py:47
  108.3 5.8 %fusion.13 = bf16[128,8,1024]{2,1,0:T(8,128)(2,1)S(1)} fusion(f32[1024,1024]{1,0:T(8,128)S(1)} %fusion.2, bf16[1024,2048]{1,0:T(8,128)(2,1)S(1)} %bitcast.112, bf16[1,2048,1024]{2,1,0:T(8,128)(2,1)S(1)} %copy-done.8), kind=kOutput, calls=%fused_computation.17 | convolution fusion | flops 4305453056 | bytes 14680064 | tf_op jit(solution)/shard_map/dot_general | solution.py:46
  114.1 5.2 %fusion.6 = bf16[128,8,2048]{2,0,1:T(8,128)(2,1)S(1)} fusion(bf16[1,1024,2048]{2,1,0:T(8,128)(2,1)S(1)} %copy-done.9, bf16[128,8,1024]{2,1,0:T(8,128)(2,1)S(1)} %fusion.13), kind=kOutput, calls=%fused_computation.11 | convolution fusion | flops 4297064448 | bytes 10485760 | tf_op jit(solution)/shard_map/dot_general | solution.py:151
  119.9 8.2 %all_to_all.50 = bf16[2,64,8,2048]{3,1,2,0:T(8,128)(2,1)} all-to-all(bf16[2,64,8,2048]{3,1,2,0:T(8,128)(2,1)S(1)} %copy.94), channel_id=1, replica_groups=mesh['sp_0'=4,'sp_1'=4,'sp_2'=4,'tp'=2] {'tp'}, dimensions={0} | all-to-all | bytes 8388608 | tf_op jit(solution)/shard_map/all_to_all | solution.py:41
  128.0 3.5 %reduce_sum.64 = bf16[64,8,2048]{2,0,1:T(8,128)(2,1)S(1)} reduce(bf16[2,64,8,2048]{3,1,2,0:T(8,128)(2,1)} %all_to_all.50, bf16[]{:T(256)} %constant.96.clone.1), dimensions={0}, to_apply=%region_7.8 | reduce | flops 1048576 | bytes 6291458 | tf_op jit(solution)/shard_map/reduce_sum | solution.py:42
  131.5 2.5 %copy.96 = bf16[64,8,2048]{2,1,0:T(8,128)(2,1)} copy(bf16[64,8,2048]{2,0,1:T(8,128)(2,1)S(1)} %reduce_sum.64) | data formatting | bytes 4194304 | tf_op jit(solution)/shard_map/reduce_sum | solution.py:42
  134.0 5.7 %all-to-all-start.6 = ((bf16[64,8,2048]{2,1,0:T(8,128)(2,1)}), bf16[64,8,2048]{2,1,0:T(8,128)(2,1)S(1)}, u32[]{:S(2)}, u32[]{:S(2)}) async-start(bf16[64,8,2048]{2,1,0:T(8,128)(2,1)} %copy.96), calls=%async_computation.6 | async-start | bytes 4194304 | tf_op jit(solution)/shard_map/all_to_all | solution.py:155
  139.7 0.7 copy.97
  140.4 29.8 %all-to-all-done.6 = bf16[64,8,2048]{2,1,0:T(8,128)(2,1)S(1)} async-done(((bf16[64,8,2048]{2,1,0:T(8,128)(2,1)}), bf16[64,8,2048]{2,1,0:T(8,128)(2,1)S(1)}, u32[]{:S(2)}, u32[]{:S(2)}) %all-to-all-start.6) | async-done | bytes 2097184 | tf_op jit(solution)/shard_map/all_to_all | solution.py:155
  170.2 1.4 gather_fusion.1
  171.6 0.7 reshape.211
  172.3 2.3 %multiply_reduce_fusion = f32[64,2048]{1,0:T(8,128)S(1)} fusion(f32[64,4,2048]{2,1,0:T(4,128)S(1)} %reshape.211, f32[64,4]{1,0:T(8,128)} %copy.97), kind=kLoop, calls=%fused_computation.16 | loop fusion | flops 917504 | bytes 2622464 | tf_op jit(solution)/shard_map/reduce_sum | solution.py:163
  174.6 0.8 fusion.24
  (64 shorter events, 7.9 us)
Async XLA Ops:
  0.0 37.2 %copy-start = (bf16[128,512]{1,0:T(8,128)(2,1)S(1)}, bf16[128,512]{1,0:T(8,128)(2,1)}, u32[]{:S(2)}) copy-start(bf16[128,512]{1,0:T(8,128)(2,1)} %param.13) | copy-start | bytes 393220
  0.0 37.0 %copy-start.3 = (bf16[128,1024]{1,0:T(8,128)(2,1)S(1)}, bf16[128,1024]{1,0:T(8,128)(2,1)}, u32[]{:S(2)}) copy-start(bf16[128,1024]{1,0:T(8,128)(2,1)} %param.16) | copy-start | bytes 786436
  7.0 42.8 %copy-start.2 = (bf16[128,1024]{1,0:T(8,128)(2,1)S(1)}, bf16[128,1024]{1,0:T(8,128)(2,1)}, u32[]{:S(2)}) copy-start(bf16[128,1024]{1,0:T(8,128)(2,1)} %param.15) | copy-start | bytes 786436
  7.0 22.3 %all-to-all-start = ((bf16[64,2,1024]{2,1,0:T(2,128)(2,1)}), bf16[64,2,1024]{2,1,0:T(2,128)(2,1)S(1)}, u32[]{:S(2)}, u32[]{:S(2)}) async-start(bf16[64,2,1024]{2,1,0:T(2,128)(2,1)} %reshape.243), calls=%async_computation | async-start | bytes 524288 | tf_op jit(solution)/shard_map/all_to_all | solution.py:22
  31.6 16.0 %all-to-all-start.1 = ((bf16[64,2,1024]{2,1,0:T(2,128)(2,1)}), bf16[64,2,1024]{2,1,0:T(2,128)(2,1)S(1)}, u32[]{:S(2)}, u32[]{:S(2)}) async-start(bf16[64,2,1024]{2,1,0:T(2,128)(2,1)} %reshape.245), calls=%async_computation.1 | async-start | bytes 524288 | tf_op jit(solution)/shard_map/all_to_all | solution.py:28
  50.7 7.4 %copy-start.4 = (bf16[64,2048]{1,0:T(8,128)(2,1)S(1)}, bf16[64,2048]{1,0:T(8,128)(2,1)}, u32[]{:S(2)}) copy-start(bf16[64,2048]{1,0:T(8,128)(2,1)} %param.18) | copy-start | bytes 786436
  50.9 7.4 %copy-start.5 = (f32[2048]{0:T(1024)S(1)}, f32[2048]{0:T(1024)}, u32[]{:S(2)}) copy-start(f32[2048]{0:T(1024)} %param.20) | copy-start | bytes 24580
  96.4 7.4 %copy-start.7 = (bf16[1,2048,1024]{2,1,0:T(8,128)(2,1)S(1)}, bf16[1,2048,1024]{2,1,0:T(8,128)(2,1)}, u32[]{:S(2)}) copy-start(bf16[1,2048,1024]{2,1,0:T(8,128)(2,1)} %param.24) | copy-start | bytes 12582916
  103.8 4.5 %copy-start.8 = (bf16[1,2048,1024]{2,1,0:T(8,128)(2,1)S(1)}, bf16[1,2048,1024]{2,1,0:T(8,128)(2,1)}, u32[]{:S(2)}) copy-start(bf16[1,2048,1024]{2,1,0:T(8,128)(2,1)} %param.23) | copy-start | bytes 12582916
  108.3 5.8 %copy-start.9 = (bf16[1,1024,2048]{2,1,0:T(8,128)(2,1)S(1)}, bf16[1,1024,2048]{2,1,0:T(8,128)(2,1)}, u32[]{:S(2)}) copy-start(bf16[1,1024,2048]{2,1,0:T(8,128)(2,1)} %param.25) | copy-start | bytes 12582916
  131.5 8.2 %copy-start.6 = (f32[64,4]{0,1:T(4,128)S(1)}, f32[64,4]{0,1:T(4,128)}, u32[]{:S(2)}) copy-start(f32[64,4]{0,1:T(4,128)} %param.22) | copy-start | bytes 3076
  134.0 36.2 %all-to-all-start.6 = ((bf16[64,8,2048]{2,1,0:T(8,128)(2,1)}), bf16[64,8,2048]{2,1,0:T(8,128)(2,1)S(1)}, u32[]{:S(2)}, u32[]{:S(2)}) async-start(bf16[64,8,2048]{2,1,0:T(8,128)(2,1)} %copy.96), calls=%async_computation.6 | async-start | bytes 4194304 | tf_op jit(solution)/shard_map/all_to_all | solution.py:155
  170.2 5.2 %copy-start.1 = (bf16[128,512]{1,0:T(8,128)(2,1)S(1)}, bf16[128,512]{1,0:T(8,128)(2,1)}, u32[]{:S(2)}) copy-start(bf16[128,512]{1,0:T(8,128)(2,1)} %param.13) | copy-start | bytes 393220
